TPU v7x, 128 devices: a whole 4x4x4 slice. The times are simulated.
128 devices in a mesh: sp: 32 (over z, y, core), tp: 4 (over x).
Axes of the slice: x: 4, y: 4, z: 4, core: 2. Of those that a mesh axis runs over, the one named last changes fastest.
Arguments:
- tokens: bfloat16 [4, 2048, 1024], P(None, 'sp', 'tp'), may hold values from -6 to 6
- norm_gain: float32 [4, 1024], replicated, may hold values from 0.1 to 1.9
- val_weight: bfloat16 [4, 1024, 512], P(None, 'sp', 'tp'), may hold values from -0.1875 to 0.1875
- gate_weight: bfloat16 [4, 1024, 512], P(None, 'sp', 'tp'), may hold values from -0.1875 to 0.1875
- conv_taps: float32 [4, 31, 512], P(None, None, 'tp'), may hold values from -1 to 1
- conv_bias: float32 [4, 512], P(None, 'tp'), may hold values from -3 to 3
- ln_gain: float32 [4, 512], P(None, 'tp'), may hold values from 0.1 to 1.9
- ln_shift: float32 [4, 512], P(None, 'tp'), may hold values from -3 to 3
- out_weight: bfloat16 [4, 512, 1024], P(None, 'tp', 'sp'), may hold values from -0.25 to 0.25
Outputs:
- stream: bfloat16 [4, 2048, 1024], P(None, 'sp', 'tp')
All inputs are finite; a program needn't handle non-finite values.
Results may differ from a plain program's by a relative error of at most 0.02.
Values may be sent and summed in bfloat16 or wider, within the bound.
A program may use at most 64 MiB of HBM per device.

v0:
```python
from functools import partial

import jax
import jax.numpy as jnp
from jax import lax
from jax.experimental import pallas as pl
from jax.experimental.pallas import tpu as pltpu
from jax.sharding import PartitionSpec as P

MESH = pl.DeviceIdType.MESH

LAYERS = 4
LAGS = (0, 1, 2, 3)


epsilon = 1e-06


def over_all(shard, axis, dim, absorb, state):
    everything = jax.tree.map(lambda a: lax.all_gather(a, axis, axis=dim, tiled=True), shard)
    return absorb(state, everything, jnp.int32(0))


def with_halo(shard, sides, width, wrap):
    for axis, dim in sides:
        size, length = lax.axis_size(axis), shard.shape[dim]
        up = [(i, (i + 1) % size) for i in range(size if wrap else size - 1)]
        down = [(j, i) for i, j in up]
        last = lax.slice_in_dim(shard, length - width, length, axis=dim)
        initial = lax.slice_in_dim(shard, 0, width, axis=dim)
        before = lax.ppermute(last, axis, up)
        after = lax.ppermute(initial, axis, down)
        shard = jnp.concatenate([before, shard, after], axis=dim)
    return shard


def over_all_2(shard, axis, dim, work):
    return work(lax.all_gather(shard, axis, axis=dim, tiled=True), jnp.int32(0))


def depthwise(padded, tap_weights, length):
    running = padded[:, 0:length] * tap_weights[0]
    for tap_idx in range(1, tap_weights.shape[0]):
        running = running + padded[:, tap_idx : tap_idx + length] * tap_weights[tap_idx]
    return running


def add_rows(left_rows, running, shard_piece, offset):
    columns = lax.dynamic_slice_in_dim(left_rows, offset, shard_piece.shape[0], 1)
    return running + jnp.dot(columns, shard_piece, preferred_element_type=jnp.float32)


def project_rows(left_rows, shard_piece, offset):
    return jnp.dot(left_rows, shard_piece, preferred_element_type=jnp.float32)


def shards(
    tokens, norm_gain, val_weight, gate_weight, conv_taps, conv_bias, ln_gain, ln_shift, out_weight
):
    stream = tokens
    num_seqs = tokens.shape[0]
    local_len = tokens.shape[1]
    chan_width = val_weight.shape[2]
    all_channels = chan_width * lax.axis_size("tp")
    half_width = conv_taps.shape[1] // 2
    for layer_idx in range(LAYERS):
        gathered = lax.all_gather(stream, "tp", axis=2, tiled=True)
        widened = gathered.astype(jnp.float32)
        scaled = widened * lax.rsqrt(jnp.mean(widened * widened, axis=-1, keepdims=True) + epsilon)
        normed = (scaled * norm_gain[layer_idx]).astype(jnp.bfloat16)
        tok_rows = normed.reshape(-1, normed.shape[2])
        zeroed = jnp.zeros((tok_rows.shape[0], chan_width), jnp.float32)
        values = over_all(val_weight[layer_idx], "sp", 0, partial(add_rows, tok_rows), zeroed)
        gates = over_all(gate_weight[layer_idx], "sp", 0, partial(add_rows, tok_rows), zeroed)
        gated = (
            (values * jax.nn.sigmoid(gates))
            .astype(jnp.bfloat16)
            .reshape(num_seqs, local_len, chan_width)
        )
        padded = with_halo(gated, (("sp", 1),), half_width, False)
        convolved = (
            depthwise(padded.astype(jnp.float32), conv_taps[layer_idx], local_len)
            + conv_bias[layer_idx]
        )
        first_sum, second_sum = lax.psum(
            (jnp.sum(convolved, axis=-1), jnp.sum(convolved * convolved, axis=-1)), "tp"
        )
        mean_val = (first_sum / all_channels)[..., None]
        spread = (second_sum / all_channels)[..., None] - mean_val * mean_val
        centered = convolved - mean_val
        normalized = (
            centered * lax.rsqrt(spread + epsilon) * ln_gain[layer_idx] + ln_shift[layer_idx]
        )
        activated = jax.nn.silu(normalized).astype(jnp.bfloat16).reshape(-1, chan_width)
        partial_terms = over_all_2(out_weight[layer_idx], "sp", 1, partial(project_rows, activated))
        full_width = partial_terms.shape[1]
        summed = lax.psum_scatter(
            partial_terms.reshape(num_seqs, local_len, full_width).astype(jnp.bfloat16),
            "tp",
            scatter_dimension=2,
            tiled=True,
        ).astype(jnp.float32)
        stream = (stream.astype(jnp.float32) + summed).astype(jnp.bfloat16)
    return stream


def stack_kernel(
    dims, tok, gain, val_w, gate_w, taps, bias, lng, lns, out_w, out,
    xs, vals, gates, outs, ptaps, pbias, plng, plns, gs, cv, act, stage,
    loc_sem, tsend, trecv, psend, precv, wsend, wrecv, osend, orecv,
):
    SP, TP, Z, L, D, C, F, W, K, TAPS, PAD, E = dims
    sp, tp = lax.axis_index("sp"), lax.axis_index("tp")
    zi, yi, xi, ci = sp // 2, sp % 2, tp // 2, tp % 2
    half = TAPS // 2

    def remote(src, dst, ss, rs, to_sp, to_tp):
        return pltpu.make_async_remote_copy(
            src_ref=src, dst_ref=dst, send_sem=ss, recv_sem=rs,
            device_id=(to_sp, to_tp), device_id_type=MESH,
        )

    def feat(t):
        return pl.ds(pl.multiple_of(t * F, F), F)

    finish = []

    def tok_copy(side, d, to_sp):
        to = lax.rem(tp + d, TP)
        rows = {0: (0, L, E), 1: (L - E, E, 0), 2: (0, E, E + L)}[side]
        return remote(
            tok.at[to, pl.ds(rows[0], rows[1]), :],
            xs.at[pl.ds(rows[2], rows[1]), feat(tp)],
            tsend.at[side, d], trecv.at[side, d], to_sp, to,
        )

    own_tok = pltpu.make_async_copy(tok.at[tp], xs.at[pl.ds(E, L), feat(tp)], loc_sem.at[0])
    own_tok.start()

    @pl.when(sp == 0)
    def _():
        xs[pl.ds(0, E), :] = jnp.zeros((E, D), xs.dtype)

    @pl.when(sp == SP - 1)
    def _():
        xs[pl.ds(E + L, E), :] = jnp.zeros((E, D), xs.dtype)

    sources = (val_w, gate_w, out_w)
    bufs = (vals, gates, outs)
    units = [(l, k, h) for l in range(LAYERS) for k in range(3) for h in range(2)]

    def block(n, zs, ys, t):
        l, k, h = units[n]
        if k < 2:
            return bufs[k].at[l, zs, ys, t, pl.ds(h * (K // 2), K // 2), :]
        rows = pl.ds(pl.multiple_of(t * W + h * (W // 2), W // 2), W // 2)
        return bufs[k].at[l, zs, ys, rows, :]

    def source(n):
        l, k, h = units[n]
        rows = sources[k].shape[1] // 2
        return sources[k].at[l, pl.ds(h * rows, rows), :]

    every = slice(None)
    sib, xpeer = xi * 2 + (1 - ci), (1 - xi) * 2 + ci
    ypeer = zi * 2 + (1 - yi)

    def y_first(n):
        return units[n][2] == 0

    own = []
    first = []
    for n in range(len(units)):
        c = pltpu.make_async_copy(source(n), block(n, zi, yi, tp), loc_sem.at[1 + n])
        own.append(c)
        first.append([
            remote(
                source(n), block(n, zi, yi, tp),
                wsend.at[n, d - 1], wrecv.at[n, d - 1], lax.rem(zi + d, Z) * 2 + yi, tp,
            )
            for d in range(1, Z)
        ])

    def start(n, slot, zs, ys, t, to_sp, to_tp):
        ref = block(n, zs, ys, t)
        c = remote(ref, ref, wsend.at[n, slot], wrecv.at[n, slot], to_sp, to_tp)
        c.start()
        finish.append(c)
        return c

    for c in own[:4]:
        c.start()
    for n in range(4):
        for c in first[n]:
            c.start()
    for d in range(1, TP):
        tok_copy(0, d, sp).start()
    small, params = [], []
    for i, (src, dst) in enumerate(((taps, ptaps), (bias, pbias), (lng, plng), (lns, plns))):
        c = pltpu.make_async_copy(src, dst.at[tp], loc_sem.at[1 + len(units) + i])
        c.start()
        small.append(c)
        for d in range(1, TP):
            r = remote(src, dst.at[tp], psend.at[i, d], precv.at[i, d], sp, lax.rem(tp + d, TP))
            r.start()
            finish.append(r)
            params.append(r)

    @pl.when(sp < SP - 1)
    def _():
        for d in range(TP):
            tok_copy(1, d, sp + 1).start()

    @pl.when(sp > 0)
    def _():
        for d in range(TP):
            tok_copy(2, d, sp - 1).start()

    for n in range(4, len(units)):
        own[n].start()
        for c in first[n]:
            c.start()

    z0 = Z - 1
    hold = {}

    def step2(n):
        own[n].wait()
        for c in first[n]:
            c.wait_recv()
            finish.append(c)
        if y_first(n):
            hold[n] = [start(n, z0, every, yi, tp, ypeer, tp)]
        else:
            hold[n] = [start(n, z0, every, yi, tp, sp, xpeer)]
        hold[n, "s"] = [start(n, z0 + 1, every, yi, tp, sp, sib)]

    def step3(n):
        for c in hold[n]:
            c.wait_recv()
        if y_first(n):
            hold[n] = [start(n, z0 + 2, every, every, tp, sp, xpeer)]
            hold[n, "s"].append(start(n, z0 + 3, every, 1 - yi, tp, sp, sib))
        else:
            hold[n] = [
                start(n, z0 + 2, every, yi, tp, ypeer, tp),
                start(n, z0 + 4, every, yi, xpeer, ypeer, tp),
            ]
            hold[n, "s"].append(start(n, z0 + 3, every, yi, xpeer, sp, sib))

    def step4(n):
        for c in hold[n]:
            c.wait_recv()
        if y_first(n):
            hold[n, "s"].append(start(n, z0 + 5, every, every, xpeer, sp, sib))
        else:
            hold[n, "s"].append(start(n, z0 + 5, every, 1 - yi, tp, sp, sib))
            hold[n, "s"].append(start(n, z0 + 6, every, 1 - yi, xpeer, sp, sib))

    def step5(n):
        for c in hold[n, "s"]:
            c.wait_recv()

    def tick(t):
        for lag, step in zip(LAGS, (step2, step3, step4, step5)):
            for h in range(2):
                if 0 <= t - lag < len(units) // 2:
                    step(2 * (t - lag) + h)

    NC = C // 128

    def gated_part(l):
        rows, base = L + 2 * E - 2 * PAD * l, PAD * l
        x = xs[pl.ds(base, rows), :].astype(jnp.float32)
        scaled = x * lax.rsqrt(jnp.mean(x * x, axis=-1, keepdims=True) + epsilon)
        normed = (scaled * gain[pl.ds(l, 1), :]).astype(jnp.bfloat16)
        place = sp * L - E + base + lax.broadcasted_iota(jnp.int32, (rows, 256), 0)
        inside = (place >= 0) & (place < SP * L)
        for j in range(C // 256):
            vw, gw = (
                jnp.concatenate([b[l, :, :, 2 * j + i].reshape(D, W) for i in range(2)], axis=1)
                for b in (vals, gates)
            )
            v = jnp.dot(normed, vw, preferred_element_type=jnp.float32)
            g = jnp.dot(normed, gw, preferred_element_type=jnp.float32)
            r = (v * jax.nn.sigmoid(g)).astype(jnp.bfloat16).astype(jnp.float32)
            r = jnp.where(inside, r, 0.0)
            gs[2 * j, pl.ds(0, rows), :] = r[:, :128]
            gs[2 * j + 1, pl.ds(0, rows), :] = r[:, 128:]

    def conv_part(l):
        rows = L + 2 * E - 2 * PAD * (l + 1)

        per = W // 128

        def one(c, carry):
            t = c // per
            lane = pl.ds(pl.multiple_of((c % per) * 128, 128), 128) if per > 1 else slice(None)
            acc = gs[c, pl.ds(PAD - half, rows), :] * ptaps[t, l, pl.ds(0, 1), lane]
            for k in range(1, TAPS):
                acc = acc + gs[c, pl.ds(PAD - half + k, rows), :] * ptaps[t, l, pl.ds(k, 1), lane]
            cv[c, pl.ds(0, rows), :] = acc + pbias[t, pl.ds(l, 1), lane]
            return carry

        lax.fori_loop(0, NC, one, 0)
        parts = [cv[c, pl.ds(0, rows), :] for c in range(NC)]
        mean = jnp.sum(sum(parts[1:], parts[0]), axis=-1, keepdims=True) / C
        cent = [p - mean for p in parts]
        sq = [p * p for p in cent]
        inv = lax.rsqrt(jnp.sum(sum(sq[1:], sq[0]), axis=-1, keepdims=True) / C + epsilon)
        for c in range(NC):
            t, lane = c // per, pl.ds((c % per) * 128, 128)
            y = cent[c] * inv * plng[t, pl.ds(l, 1), lane] + plns[t, pl.ds(l, 1), lane]
            act[pl.ds(0, rows), pl.ds(c * 128, 128)] = (y * jax.nn.sigmoid(y)).astype(jnp.bfloat16)

    def out_part(l):
        rows, base = L + 2 * E - 2 * PAD * (l + 1), PAD * (l + 1)
        a = act[pl.ds(0, rows), :]
        for z in range(Z):
            w = jnp.concatenate([outs[l, z, 0], outs[l, z, 1]], axis=1)
            y = jnp.dot(a, w, preferred_element_type=jnp.float32)
            cols = pl.ds(z * 2 * K, 2 * K)
            s = xs[pl.ds(base, rows), cols].astype(jnp.float32)
            xs[pl.ds(base, rows), cols] = (s + y).astype(jnp.bfloat16)

    def arrived():
        own_tok.wait()
        for d in range(1, TP):
            c = tok_copy(0, d, sp)
            c.wait_recv()
            finish.append(c)
        for c in small:
            c.wait()
        for c in params:
            c.wait_recv()

        @pl.when(sp > 0)
        def _():
            for d in range(TP):
                tok_copy(1, d, sp).wait_recv()

        @pl.when(sp < SP - 1)
        def _():
            for d in range(TP):
                tok_copy(2, d, sp).wait_recv()

    t, last = 0, LAGS[-1]
    for l in range(LAYERS):
        while t <= 3 * l + 1 + last:
            tick(t)
            t += 1
        if l == 0:
            arrived()
        gated_part(l)
        tick(t)
        t += 1
        conv_part(l)
        if l + 1 < LAYERS:
            tick(t)
            t += 1
        out_part(l)

    sends = []
    for d in range(1, TP):
        to = lax.rem(tp + d, TP)
        c = remote(
            xs.at[pl.ds(E, L), feat(to)], out.at[tp],
            osend.at[d], orecv.at[d], sp, to,
        )
        c.start()
        sends.append(c)
    mine = pltpu.make_async_copy(xs.at[pl.ds(E, L), feat(tp)], out.at[tp], loc_sem.at[0])
    mine.start()
    for c in finish:
        c.wait_send()

    @pl.when(sp < SP - 1)
    def _():
        for d in range(TP):
            tok_copy(1, d, sp).wait_send()

    @pl.when(sp > 0)
    def _():
        for d in range(TP):
            tok_copy(2, d, sp).wait_send()

    mine.wait()
    for c in sends:
        c.wait()


def stacked(tokens, norm_gain, val_weight, gate_weight, conv_taps, conv_bias, ln_gain, ln_shift, out_weight):
    SP, TP = lax.axis_size("sp"), lax.axis_size("tp")
    seqs, L, F = tokens.shape
    D = F * TP
    layers, K, W = val_weight.shape
    C = W * TP
    TAPS = conv_taps.shape[1]
    PAD = -(-(TAPS // 2) // 16) * 16
    E = PAD * LAYERS
    Z = SP // 2
    rows = L + 2 * E
    vmem = pl.BlockSpec(memory_space=pltpu.VMEM)
    bf16, f32 = jnp.bfloat16, jnp.float32
    dma = pltpu.SemaphoreType.DMA
    units = 6 * LAYERS
    return pl.pallas_call(
        partial(stack_kernel, (SP, TP, Z, L, D, C, F, W, K, TAPS, PAD, E)),
        out_shape=jax.ShapeDtypeStruct(tokens.shape, tokens.dtype),
        in_specs=[vmem] * 9,
        out_specs=vmem,
        scratch_shapes=[
            pltpu.VMEM((rows, D), bf16),
            pltpu.VMEM((LAYERS, Z, 2, TP, K, W), bf16),
            pltpu.VMEM((LAYERS, Z, 2, TP, K, W), bf16),
            pltpu.VMEM((LAYERS, Z, 2, C, K), bf16),
            pltpu.VMEM((TP,) + conv_taps.shape, f32),
            pltpu.VMEM((TP,) + conv_bias.shape, f32),
            pltpu.VMEM((TP,) + conv_bias.shape, f32),
            pltpu.VMEM((TP,) + conv_bias.shape, f32),
            pltpu.VMEM((C // 128, rows, 128), f32),
            pltpu.VMEM((C // 128, rows, 128), f32),
            pltpu.VMEM((rows, C), bf16),
            pltpu.VMEM((8, 128), f32),
            dma((1 + units + 4,)),
            dma((3, TP)), dma((3, TP)),
            dma((4, TP)), dma((4, TP)),
            dma((units, Z + 6)), dma((units, Z + 6)),
            dma((TP,)), dma((TP,)),
        ],
        compiler_params=pltpu.CompilerParams(has_side_effects=True, vmem_limit_bytes=48 * 1024 * 1024),
        name="stack",
    )(tokens, norm_gain, val_weight, gate_weight, conv_taps, conv_bias, ln_gain, ln_shift, out_weight)


def fits(tokens, val_weight, conv_taps):
    SP, TP = lax.axis_size("sp"), lax.axis_size("tp")
    seqs, L, F = tokens.shape
    layers, K, W = val_weight.shape
    halo = -(-(conv_taps.shape[1] // 2) // 16) * 16 * LAYERS
    return (
        TP == 4 and SP % 2 == 0 and seqs == TP and L >= halo and L % 16 == 0
        and F % 128 == 0 and K % 128 == 0 and W == 128 and layers == LAYERS
    )


def either(tokens, norm_gain, val_weight, gate_weight, conv_taps, *rest):
    work = stacked if fits(tokens, val_weight, conv_taps) else shards
    return work(tokens, norm_gain, val_weight, gate_weight, conv_taps, *rest)


def solution(mesh):
    placed = (
        P(None, "sp", "tp"),
        P(),
        P(None, "sp", "tp"),
        P(None, "sp", "tp"),
        P(None, None, "tp"),
        P(None, "tp"),
        P(None, "tp"),
        P(None, "tp"),
        P(None, "tp", "sp"),
    )
    return jax.shard_map(
        either, mesh=mesh, in_specs=placed, out_specs=P(None, "sp", "tp"), check_vma=False
    )
```

profile of v0, /device:TPU:0, one launch (start us, length us, event | category | flops | bytes accessed | tf_op | source)
XLA Modules:
  0.0 452.4 jit_solution(8214869156785381920)
XLA Ops:
  6.5 0.9 fusion.211
  7.4 13.5 %all_gather.48 = bf16[4,64,1024]{2,1,0:T(8,128)(2,1)S(1)} all-gather(bf16[4,64,256]{2,1,0:T(8,128)(2,1)} %param.9), channel_id=1, replica_groups=mesh['sp'=32,'tp'=4] {'tp'}, dimensions={2}, use_global_device_ids=true | all-gather | bytes 655360 | tf_op jit(solution)/shard_map/all_gather | solution.py:67
  21.1 0.6 copy-done.2
  21.7 26.3 %all-gather = bf16[1,1024,128]{2,1,0:T(8,128)(2,1)S(1)} all-gather(bf16[1,32,128]{2,1,0:T(8,128)(2,1)S(1)} %get-tuple-element.163), channel_id=2, replica_groups=mesh['sp'=32,'tp'=4] {'sp'}, dimensions={1}, use_global_device_ids=true | all-gather | bytes 270336 | tf_op jit(solution)/shard_map/all_gather | solution.py:20
  48.0 24.1 %all-gather.1 = bf16[1,1024,128]{2,1,0:T(8,128)(2,1)S(1)} all-gather(bf16[1,32,128]{2,1,0:T(8,128)(2,1)S(1)} %get-tuple-element.159), channel_id=3, replica_groups=mesh['sp'=32,'tp'=4] {'sp'}, dimensions={1}, use_global_device_ids=true | all-gather | bytes 270336 | tf_op jit(solution)/shard_map/all_gather | solution.py:20
  72.6 0.3 fusion.16
  72.9 2.3 collective-permute-start
  75.2 1.3 collective-permute-start.1
  76.6 0.7 copy-done.5
  77.3 0.7 copy-done.6
  77.9 26.5 %all-gather.2 = bf16[1,128,1024]{1,2,0:T(8,128)(2,1)S(1)} all-gather(bf16[1,128,32]{1,2,0:T(8,128)(2,1)S(1)} %get-tuple-element.165), channel_id=4, replica_groups=mesh['sp'=32,'tp'=4] {'sp'}, dimensions={2}, use_global_device_ids=true | all-gather | bytes 270336 | tf_op jit(solution)/shard_map/all_gather | solution.py:38
  104.4 0.6 fusion.199
  105.0 10.7 %all-reduce.3 = (f32[4,64]{1,0:T(4,128)S(1)}, f32[4,64]{1,0:T(4,128)S(1)}) all-reduce(f32[4,64]{1,0:T(4,128)S(1)} %get-tuple-element.12, f32[4,64]{1,0:T(4,128)S(1)} %get-tuple-element.11), channel_id=1, replica_groups=mesh['sp'=32,'tp'=4] {'tp'}, use_global_device_ids=true, to_apply=%region_4.0 | all-reduce | flops 512 | bytes 4096 | tf_op jit(solution)/shard_map/psum | solution.py:85
  115.7 1.2 convolution_convert_fusion.3
  117.0 22.9 %all-gather.3 = bf16[1,1024,128]{2,1,0:T(8,128)(2,1)S(1)} all-gather(bf16[1,32,128]{2,1,0:T(8,128)(2,1)S(1)} %get-tuple-element.162), channel_id=5, replica_groups=mesh['sp'=32,'tp'=4] {'sp'}, dimensions={1}, use_global_device_ids=true | all-gather | bytes 270336 | tf_op jit(solution)/shard_map/all_gather | solution.py:20
  139.9 23.7 %all-gather.4 = bf16[1,1024,128]{2,1,0:T(8,128)(2,1)S(1)} all-gather(bf16[1,32,128]{2,1,0:T(8,128)(2,1)S(1)} %get-tuple-element.158), channel_id=6, replica_groups=mesh['sp'=32,'tp'=4] {'sp'}, dimensions={1}, use_global_device_ids=true | all-gather | bytes 270336 | tf_op jit(solution)/shard_map/all_gather | solution.py:20
  163.6 0.9 add_convert_fusion.3
  164.6 13.5 %all_gather.52 = bf16[4,64,1024]{2,1,0:T(8,128)(2,1)S(1)} all-gather(bf16[4,64,256]{2,1,0:T(8,128)(2,1)S(1)} %add_convert_fusion.3), channel_id=1, replica_groups=mesh['sp'=32,'tp'=4] {'tp'}, dimensions={2}, use_global_device_ids=true | all-gather | bytes 655360 | tf_op jit(solution)/shard_map/all_gather | solution.py:67
  178.8 0.3 fusion.17
  179.1 1.3 collective-permute-start.2
  180.4 1.3 collective-permute-start.3
  181.7 28.2 %all-gather.5 = bf16[1,128,1024]{1,2,0:T(8,128)(2,1)S(1)} all-gather(bf16[1,128,32]{1,2,0:T(8,128)(2,1)S(1)} %get-tuple-element.166), channel_id=7, replica_groups=mesh['sp'=32,'tp'=4] {'sp'}, dimensions={2}, use_global_device_ids=true | all-gather | bytes 270336 | tf_op jit(solution)/shard_map/all_gather | solution.py:38
  209.9 0.6 fusion.198
  210.5 7.7 %all-reduce.2 = (f32[4,64]{1,0:T(4,128)S(1)}, f32[4,64]{1,0:T(4,128)S(1)}) all-reduce(f32[4,64]{1,0:T(4,128)S(1)} %get-tuple-element.10, f32[4,64]{1,0:T(4,128)S(1)} %get-tuple-element.9), channel_id=1, replica_groups=mesh['sp'=32,'tp'=4] {'tp'}, use_global_device_ids=true, to_apply=%region_10.11 | all-reduce | flops 512 | bytes 4096 | tf_op jit(solution)/shard_map/psum | solution.py:85
  218.2 1.2 convolution_convert_fusion.2
  219.5 22.4 %all-gather.6 = bf16[1,1024,128]{2,1,0:T(8,128)(2,1)S(1)} all-gather(bf16[1,32,128]{2,1,0:T(8,128)(2,1)S(1)} %get-tuple-element.164), channel_id=8, replica_groups=mesh['sp'=32,'tp'=4] {'sp'}, dimensions={1}, use_global_device_ids=true | all-gather | bytes 270336 | tf_op jit(solution)/shard_map/all_gather | solution.py:20
  241.8 24.1 %all-gather.7 = bf16[1,1024,128]{2,1,0:T(8,128)(2,1)S(1)} all-gather(bf16[1,32,128]{2,1,0:T(8,128)(2,1)S(1)} %get-tuple-element.160), channel_id=9, replica_groups=mesh['sp'=32,'tp'=4] {'sp'}, dimensions={1}, use_global_device_ids=true | all-gather | bytes 270336 | tf_op jit(solution)/shard_map/all_gather | solution.py:20
  266.0 0.9 add_convert_fusion.2
  266.9 12.9 %all_gather.56 = bf16[4,64,1024]{2,1,0:T(8,128)(2,1)S(1)} all-gather(bf16[4,64,256]{2,1,0:T(8,128)(2,1)S(1)} %add_convert_fusion.2), channel_id=1, replica_groups=mesh['sp'=32,'tp'=4] {'tp'}, dimensions={2}, use_global_device_ids=true | all-gather | bytes 655360 | tf_op jit(solution)/shard_map/all_gather | solution.py:67
  280.5 0.3 fusion.18
  280.8 1.3 collective-permute-start.4
  282.1 1.3 collective-permute-start.5
  283.4 27.4 %all-gather.8 = bf16[1,128,1024]{1,2,0:T(8,128)(2,1)S(1)} all-gather(bf16[1,128,32]{1,2,0:T(8,128)(2,1)S(1)} %get-tuple-element.168), channel_id=10, replica_groups=mesh['sp'=32,'tp'=4] {'sp'}, dimensions={2}, use_global_device_ids=true | all-gather | bytes 270336 | tf_op jit(solution)/shard_map/all_gather | solution.py:38
  310.9 0.6 fusion.197
  311.5 9.9 %all-reduce.1 = (f32[4,64]{1,0:T(4,128)S(1)}, f32[4,64]{1,0:T(4,128)S(1)}) all-reduce(f32[4,64]{1,0:T(4,128)S(1)} %get-tuple-element.8, f32[4,64]{1,0:T(4,128)S(1)} %get-tuple-element.7), channel_id=1, replica_groups=mesh['sp'=32,'tp'=4] {'tp'}, use_global_device_ids=true, to_apply=%region_16.17 | all-reduce | flops 512 | bytes 4096 | tf_op jit(solution)/shard_map/psum | solution.py:85
  321.4 1.2 convolution_convert_fusion.1
  322.7 22.9 %all-gather.9 = bf16[1,1024,128]{2,1,0:T(8,128)(2,1)S(1)} all-gather(bf16[1,32,128]{2,1,0:T(8,128)(2,1)S(1)} %get-tuple-element.161), channel_id=11, replica_groups=mesh['sp'=32,'tp'=4] {'sp'}, dimensions={1}, use_global_device_ids=true | all-gather | bytes 270336 | tf_op jit(solution)/shard_map/all_gather | solution.py:20
  345.6 23.8 %all-gather.10 = bf16[1,1024,128]{2,1,0:T(8,128)(2,1)S(1)} all-gather(bf16[1,32,128]{2,1,0:T(8,128)(2,1)S(1)} %get-tuple-element.157), channel_id=12, replica_groups=mesh['sp'=32,'tp'=4] {'sp'}, dimensions={1}, use_global_device_ids=true | all-gather | bytes 270336 | tf_op jit(solution)/shard_map/all_gather | solution.py:20
  369.4 0.9 add_convert_fusion.1
  370.3 13.5 %all_gather.60 = bf16[4,64,1024]{2,1,0:T(8,128)(2,1)S(1)} all-gather(bf16[4,64,256]{2,1,0:T(8,128)(2,1)S(1)} %add_convert_fusion.1), channel_id=1, replica_groups=mesh['sp'=32,'tp'=4] {'tp'}, dimensions={2}, use_global_device_ids=true | all-gather | bytes 655360 | tf_op jit(solution)/shard_map/all_gather | solution.py:67
  384.9 1.3 collective-permute-start.6
  386.2 1.3 collective-permute-start.7
  387.5 28.0 %all-gather.11 = bf16[1,128,1024]{1,2,0:T(8,128)(2,1)S(1)} all-gather(bf16[1,128,32]{1,2,0:T(8,128)(2,1)S(1)} %get-tuple-element.167), channel_id=13, replica_groups=mesh['sp'=32,'tp'=4] {'sp'}, dimensions={2}, use_global_device_ids=true | all-gather | bytes 270336 | tf_op jit(solution)/shard_map/all_gather | solution.py:38
  415.5 0.6 fusion.196
  416.1 7.7 %all-reduce = (f32[4,64]{1,0:T(4,128)S(1)}, f32[4,64]{1,0:T(4,128)S(1)}) all-reduce(f32[4,64]{1,0:T(4,128)S(1)} %get-tuple-element.6, f32[4,64]{1,0:T(4,128)S(1)} %get-tuple-element.5), channel_id=1, replica_groups=mesh['sp'=32,'tp'=4] {'tp'}, use_global_device_ids=true, to_apply=%region_22.23 | all-reduce | flops 512 | bytes 4096 | tf_op jit(solution)/shard_map/psum | solution.py:85
  423.8 1.2 convolution_convert_fusion
  425.0 19.3 %reduce-scatter.11.cloned.1.call-done = bf16[4,64,256]{2,1,0:T(8,128)(2,1)} async-done(((bf16[4,64,1024]{2,1,0:T(8,128)(2,1)}), bf16[4,64,256]{2,1,0:T(8,128)(2,1)}) %reduce-scatter.11.cloned.1.call-update) | async-done | bytes 131088 | tf_op jit(solution)/shard_map/reduce_scatter | solution.py:97
  444.3 1.6 add_convert_fusion
  (73 shorter events, 3.6 us)
Async XLA Ops:
  6.5 157.1 %reduce-scatter.5.cloned.1.call-start = ((), (), s32[]{:S(2)}) async-start(), calls=%async_computation.4 | async-start | bytes 655360 | tf_op jit(solution)/shard_map/reduce_scatter | solution.py:97
  20.9 0.8 copy-start.2
  21.7 26.3 %copy-start.3 = (bf16[4,32,128]{2,1,0:T(8,128)(2,1)S(1)}, bf16[4,32,128]{2,1,0:T(8,128)(2,1)}, u32[]{:S(2)}) copy-start(bf16[4,32,128]{2,1,0:T(8,128)(2,1)} %param.12) | copy-start | bytes 98308
  72.9 3.6 copy-start.1
  72.9 4.3 copy-start.4
  72.9 31.5 %collective-permute-start = (bf16[4,15,128]{2,1,0:T(8,128)(2,1)S(1)}, bf16[4,15,128]{2,1,0:T(8,128)(2,1)S(1)}, u32[]{:S(2)}, u32[]{:S(2)}) collective-permute-start(bf16[4,15,128]{2,1,0:T(8,128)(2,1)S(1)} %get-tuple-element.31), channel_id=1, source_target_pairs={{0,4},{4,8},{8,12},{12,16},{16,20},{20,24},{24,28},{28,32},{32,36}... | collective-permute-start | bytes 46088 | tf_op jit(solution)/shard_map/ppermute | solution.py:31
  75.2 29.2 %collective-permute-start.1 = (bf16[4,15,128]{2,1,0:T(8,128)(2,1)S(1)}, bf16[4,15,128]{2,1,0:T(8,128)(2,1)S(1)}, u32[]{:S(2)}, u32[]{:S(2)}) collective-permute-start(bf16[4,15,128]{2,1,0:T(8,128)(2,1)S(1)} %get-tuple-element.32), channel_id=1, source_target_pairs={{4,0},{8,4},{12,8},{16,12},{20,16},{24,20},{28,24},{32,28},{36,32}... | collective-permute-start | bytes 46088 | tf_op jit(solution)/shard_map/ppermute | solution.py:32
  76.5 0.7 copy-start.5
  77.2 0.7 copy-start.6
  77.2 0.7 copy-start.7
  116.9 149.1 %reduce-scatter.7.cloned.1.call-start = ((), (), s32[]{:S(2)}) async-start(), calls=%async_computation.5 | async-start | bytes 655360 | tf_op jit(solution)/shard_map/reduce_scatter | solution.py:97
  139.9 23.7 %copy-start = (bf16[4,64,256]{2,1,0:T(8,128)(2,1)S(1)}, bf16[4,64,256]{2,1,0:T(8,128)(2,1)}, u32[]{:S(2)}) copy-start(bf16[4,64,256]{2,1,0:T(8,128)(2,1)} %param.9) | copy-start | bytes 393220
  179.1 30.8 %collective-permute-start.2 = (bf16[4,15,128]{2,1,0:T(8,128)(2,1)S(1)}, bf16[4,15,128]{2,1,0:T(8,128)(2,1)S(1)}, u32[]{:S(2)}, u32[]{:S(2)}) collective-permute-start(bf16[4,15,128]{2,1,0:T(8,128)(2,1)S(1)} %get-tuple-element.29), channel_id=1, source_target_pairs={{0,4},{4,8},{8,12},{12,16},{16,20},{20,24},{24,28},{28,32},{32,36}... | collective-permute-start | bytes 46088 | tf_op jit(solution)/shard_map/ppermute | solution.py:31
  180.4 29.5 %collective-permute-start.3 = (bf16[4,15,128]{2,1,0:T(8,128)(2,1)S(1)}, bf16[4,15,128]{2,1,0:T(8,128)(2,1)S(1)}, u32[]{:S(2)}, u32[]{:S(2)}) collective-permute-start(bf16[4,15,128]{2,1,0:T(8,128)(2,1)S(1)} %get-tuple-element.30), channel_id=1, source_target_pairs={{4,0},{8,4},{12,8},{16,12},{20,16},{24,20},{28,24},{32,28},{36,32}... | collective-permute-start | bytes 46088 | tf_op jit(solution)/shard_map/ppermute | solution.py:32
  219.4 150.0 %reduce-scatter.9.cloned.1.call-start = ((), (), s32[]{:S(2)}) async-start(), calls=%async_computation.6 | async-start | bytes 655360 | tf_op jit(solution)/shard_map/reduce_scatter | solution.py:97
  280.8 30.0 %collective-permute-start.4 = (bf16[4,15,128]{2,1,0:T(8,128)(2,1)S(1)}, bf16[4,15,128]{2,1,0:T(8,128)(2,1)S(1)}, u32[]{:S(2)}, u32[]{:S(2)}) collective-permute-start(bf16[4,15,128]{2,1,0:T(8,128)(2,1)S(1)} %get-tuple-element.27), channel_id=1, source_target_pairs={{0,4},{4,8},{8,12},{12,16},{16,20},{20,24},{24,28},{28,32},{32,36}... | collective-permute-start | bytes 46088 | tf_op jit(solution)/shard_map/ppermute | solution.py:31
  282.1 28.8 %collective-permute-start.5 = (bf16[4,15,128]{2,1,0:T(8,128)(2,1)S(1)}, bf16[4,15,128]{2,1,0:T(8,128)(2,1)S(1)}, u32[]{:S(2)}, u32[]{:S(2)}) collective-permute-start(bf16[4,15,128]{2,1,0:T(8,128)(2,1)S(1)} %get-tuple-element.28), channel_id=1, source_target_pairs={{4,0},{8,4},{12,8},{16,12},{20,16},{24,20},{28,24},{32,28},{36,32}... | collective-permute-start | bytes 46088 | tf_op jit(solution)/shard_map/ppermute | solution.py:32
  322.6 121.7 %reduce-scatter.11.cloned.1.call-start = ((), (), s32[]{:S(2)}) async-start(), calls=%async_computation.7 | async-start | bytes 655360 | tf_op jit(solution)/shard_map/reduce_scatter | solution.py:97
  384.9 30.6 %collective-permute-start.6 = (bf16[4,15,128]{2,1,0:T(8,128)(2,1)S(1)}, bf16[4,15,128]{2,1,0:T(8,128)(2,1)S(1)}, u32[]{:S(2)}, u32[]{:S(2)}) collective-permute-start(bf16[4,15,128]{2,1,0:T(8,128)(2,1)S(1)} %get-tuple-element.25), channel_id=1, source_target_pairs={{0,4},{4,8},{8,12},{12,16},{16,20},{20,24},{24,28},{28,32},{32,36}... | collective-permute-start | bytes 46088 | tf_op jit(solution)/shard_map/ppermute | solution.py:31
  386.2 29.3 %collective-permute-start.7 = (bf16[4,15,128]{2,1,0:T(8,128)(2,1)S(1)}, bf16[4,15,128]{2,1,0:T(8,128)(2,1)S(1)}, u32[]{:S(2)}, u32[]{:S(2)}) collective-permute-start(bf16[4,15,128]{2,1,0:T(8,128)(2,1)S(1)} %get-tuple-element.26), channel_id=1, source_target_pairs={{4,0},{8,4},{12,8},{16,12},{20,16},{24,20},{28,24},{32,28},{36,32}... | collective-permute-start | bytes 46088 | tf_op jit(solution)/shard_map/ppermute | solution.py:32
Sparse Core Ops, SparseCore 0:
  117.0 18.5 reduce-scatter.4
  219.5 19.1 reduce-scatter.6
  322.7 18.5 reduce-scatter.8
  425.1 19.0 reduce-scatter.10
where the time goes:
time: 453 us; the launch traced here: 452 us
  blocking collectives  390 us (86%)
  waiting for transfers between devices  19.4 us (4%)
  between operations  13.5 us (3%)
  starting transfers between devices  11.4 us (3%)
  other arithmetic  8.33 us (2%)
  matrix products  7 us (2%)
    all_gather x8, blocking collectives, over_all(): lax.all_gather(a, axis, axis=dim, tiled=True)  190 us
    all_gather x4, blocking collectives, over_all_2(): return work(lax.all_gather(shard, axis, axis=dim, tiled=True), jnp.int32(0))  110 us
    all_gather x4, blocking collectives, shards(): gathered = lax.all_gather(stream, 'tp', axis=2, tiled=True)  53.4 us
    psum x4, blocking collectives, shards(): lax.psum((jnp.sum(convolved, axis=-1), jnp.sum(convolved * convolved, axi...  36.1 us
    reduce_scatter x4, waiting for transfers between devices, shards(): lax.psum_scatter(partial_terms.reshape(num_seqs, local_len, full_width).a...  19.3 us
  transfers between devices with their start and end apart: 12, of which 1 were waited for; matrix products, arithmetic and copies ran while one was open for 0% of the time, Pallas kernels for 0%

commit v1 on v0

v1 whole, which is shorter than its diff:
```python
from functools import partial

import jax
import jax.numpy as jnp
from jax import lax
from jax.experimental import pallas as pl
from jax.experimental.pallas import tpu as pltpu
from jax.sharding import PartitionSpec as P

MESH = pl.DeviceIdType.MESH
epsilon = 1e-06

N = 4
ORDERS = (("x", "y", "z"), ("y", "z", "x"), ("z", "x", "y"))
ALL = slice(None)


def stack_kernel(
    dims, tok_h, gain_h, val_h, gate_h, taps_h, bias_h, lng_h, lns_h, outw_h, out,
    xs, wv, wg, wo, tokb, gain, ptaps, pbias, plng, plns, ow, gs, cv, act, fin,
    loc, tsend, trecv, hsend, hrecv, psend, precv, qsend, qrecv,
    as_, ar, bs, br, cs, cr, fs, fr, ss, sr, osend, orecv,
):
    LAYERS, L, D, C, F, K, TAPS, PAD, E = dims
    SP, TP = lax.axis_size("sp"), lax.axis_size("tp")
    sp, tp = lax.axis_index("sp"), lax.axis_index("tp")
    half = TAPS // 2
    me = {"x": tp, "y": lax.rem(sp // 2, N), "z": sp // (2 * N)}
    core = lax.rem(sp, 2)
    W = (wv, wg, wo)

    def device(at, c=None):
        return (at["z"] * (2 * N) + at["y"] * 2 + (core if c is None else c), at["x"])

    def along(dim, d):
        return lax.rem(me[dim] + d + N, N)

    def neighbour(dim, d):
        return device({**me, dim: along(dim, d)})

    sibling = device(me, 1 - core)
    before = (lax.rem(sp + SP - 1, SP), tp)
    after = (lax.rem(sp + 1, SP), tp)

    def remote(src, dst, ss_, rs_, to):
        return pltpu.make_async_remote_copy(
            src_ref=src, dst_ref=dst, send_sem=ss_, recv_sem=rs_,
            device_id=to, device_id_type=MESH,
        )

    def block(k, l, at, rows=ALL):
        return W[k].at[l, at["x"], at["z"], at["y"], core, rows, :]

    started = []

    def go(c):
        c.start()
        started.append(c)
        return c

    def load(src, dst, i):
        c = pltpu.make_async_copy(src, dst, loc.at[i])
        c.start()
        return c

    own_out = load(outw_h, ow, 0)
    every = pl.ds(0, LAYERS)
    own_val = load(val_h, block(0, every, me), 1)
    own_gate = load(gate_h, block(1, every, me), 2)
    own_tok = load(tok_h, tokb, 3)

    def feat(t):
        return pl.ds(pl.multiple_of(t * F, F), F)

    own_x = load(tok_h.at[tp], xs.at[pl.ds(E, L), feat(tp)], 4)
    small_src = (bias_h, lng_h, lns_h)
    small_dst = (pbias, plng, plns)
    own_small = [load(taps_h, ptaps.at[tp], 5)]
    own_small += [load(s, d.at[tp], 6 + i) for i, (s, d) in enumerate(zip(small_src, small_dst))]
    own_gain = load(gain_h, gain, 9)

    barrier = pltpu.get_barrier_semaphore()
    peers = [neighbour(dim, d) for dim in "xyz" for d in (1, 2, 3)] + [before, after, sibling]
    for p in peers:
        pl.semaphore_signal(barrier, inc=1, device_id=p, device_id_type=MESH)

    own_out.wait()
    for l in range(LAYERS):
        piece = jnp.transpose(ow[l].astype(jnp.float32)).astype(jnp.bfloat16)
        wo[pl.ds(l, 1), pl.ds(me["x"], 1), pl.ds(me["z"], 1), pl.ds(me["y"], 1), pl.ds(core, 1)] = (
            piece.reshape(1, 1, 1, 1, 1, K, 128)
        )
    own_val.wait()
    own_gate.wait()
    own_tok.wait()
    pl.semaphore_wait(barrier, len(peers))

    JUMPS = (1, -1, 2)

    def first(k, g):
        ref = block(k, 0 if g == 0 else pl.ds(1, LAYERS - 1), me)
        return [
            remote(ref, ref, as_.at[k, g, j], ar.at[k, g, j], neighbour(ORDERS[k][0], d))
            for j, d in enumerate(JUMPS)
        ]

    def second(k, l):
        ref = block(k, l, {**me, ORDERS[k][0]: ALL})
        return [
            remote(ref, ref, bs.at[k, l, j], br.at[k, l, j], neighbour(ORDERS[k][1], d))
            for j, d in enumerate(JUMPS)
        ]

    def plane(k, i, d, rows=ALL):
        a, b, e = ORDERS[k]
        at = {a: ALL, b: pl.ds(2 * (i % 2), 2), e: along(e, d) if d else me[e]}
        return block(k, i // 2, at, rows)

    def third(k, i):
        ref = plane(k, i, 0)
        return [
            remote(ref, ref, cs.at[k, i, j], cr.at[k, i, j], neighbour(ORDERS[k][2], d))
            for j, d in enumerate((1, -1))
        ]

    def fourth(k, i):
        res = []
        for j, d in enumerate((1, -1)):
            ref = plane(k, i, -d, pl.ds(j * (K // 2), K // 2))
            res.append(
                remote(ref, ref, fs.at[k, i, j], fr.at[k, i, j], neighbour(ORDERS[k][2], d))
            )
        return res

    def across(k, i, q):
        ref = plane(k, i, (0, -1, 1, 2)[q])
        return remote(ref, ref, ss.at[k, i, q], sr.at[k, i, q], sibling)

    def send(copies):
        for c in copies:
            go(c)

    def land(copies):
        for c in copies:
            c.wait_recv()

    def open_chunk(k, i):
        send(third(k, i))
        go(across(k, i, 0))

    def advance(k, i):
        if i < 2 * LAYERS:
            land(third(k, i))
            send(fourth(k, i))
            go(across(k, i, 1))
            go(across(k, i, 2))
        if i > 0:
            land(fourth(k, i - 1))
            go(across(k, i - 1, 3))
        if i % 2 == 0:
            l = i // 2 + 1
            if l < LAYERS:
                land(second(k, l))
                open_chunk(k, 2 * l)
                open_chunk(k, 2 * l + 1)
        elif (i + 1) // 2 + 1 < LAYERS:
            send(second(k, (i + 1) // 2 + 1))

    def tick(i):
        for k in range(3):
            advance(k, i)

    def complete(k, l):
        for i in (2 * l, 2 * l + 1):
            land([across(k, i, q) for q in range(4)])

    for k in range(3):
        send(first(k, 0))

    def tok_copy(d):
        to = lax.rem(tp + d, TP)
        return remote(
            tokb.at[to], xs.at[pl.ds(E, L), feat(tp)], tsend.at[d], trecv.at[d], (sp, to)
        )

    tok_copies = [tok_copy(d) for d in range(1, TP)]
    send(tok_copies)
    for k in range(3):
        send(first(k, 1))
    for k in range(3):
        land(first(k, 0))
        send(second(k, 0))
    own_x.wait()
    land(tok_copies)
    to_before = remote(
        xs.at[pl.ds(E, L)], xs.at[pl.ds(E + L, L)], hsend.at[0], hrecv.at[0], before
    )
    to_after = remote(xs.at[pl.ds(E, L)], xs.at[pl.ds(0, L)], hsend.at[1], hrecv.at[1], after)

    @pl.when(sp > 0)
    def _():
        to_before.start()

    @pl.when(sp < SP - 1)
    def _():
        to_after.start()

    @pl.when(sp == 0)
    def _():
        xs[pl.ds(0, E), :] = jnp.zeros((E, D), xs.dtype)

    @pl.when(sp == SP - 1)
    def _():
        xs[pl.ds(E + L, E), :] = jnp.zeros((E, D), xs.dtype)

    for k in range(3):
        land(first(k, 1))
    for k in range(3):
        land(second(k, 0))
        open_chunk(k, 0)
        open_chunk(k, 1)
        send(second(k, 1))

    for c in own_small:
        c.wait()
    pair = pl.ds(core * (LAYERS // 2), LAYERS // 2)

    def taps_copy(d):
        ref = ptaps.at[tp, pair]
        return remote(ref, ref, psend.at[0, d], precv.at[0, d], (sp, lax.rem(tp + d, TP)))

    def taps_across(d):
        ref = ptaps.at[lax.rem(tp + d, TP), pair]
        return remote(ref, ref, qsend.at[d], qrecv.at[d], sibling)

    def small_copy(i, d):
        ref = small_dst[i].at[tp]
        return remote(ref, ref, psend.at[1 + i, d], precv.at[1 + i, d], (sp, lax.rem(tp + d, TP)))

    tap_copies = [taps_copy(d) for d in range(1, TP)]
    small_copies = [small_copy(i, d) for i in range(3) for d in range(1, TP)]
    tap_crossings = [taps_across(d) for d in range(1, TP)]
    send(tap_copies)
    send(small_copies)

    NC = C // 128

    def gated_part(l):
        rows, base = L + 2 * E - 2 * PAD * l, PAD * l
        x = xs[pl.ds(base, rows), :].astype(jnp.float32)
        scaled = x * lax.rsqrt(jnp.mean(x * x, axis=-1, keepdims=True) + epsilon)
        normed = (scaled * gain[pl.ds(l, 1), :]).astype(jnp.bfloat16)
        place = sp * L - E + base + lax.broadcasted_iota(jnp.int32, (rows, 128), 0)
        inside = (place >= 0) & (place < SP * L)
        for t in range(NC):
            w = jnp.concatenate([wv[l, t].reshape(D, 128), wg[l, t].reshape(D, 128)], axis=1)
            both = jnp.dot(normed, w, preferred_element_type=jnp.float32)
            v, g = both[:, :128], both[:, 128:]
            r = (v * jax.nn.sigmoid(g)).astype(jnp.bfloat16).astype(jnp.float32)
            gs[t, pl.ds(0, rows), :] = jnp.where(inside, r, 0.0)

    def conv_part(l):
        rows = L + 2 * E - 2 * PAD * (l + 1)

        def one(c, carry):
            acc = gs[c, pl.ds(PAD - half, rows), :] * ptaps[c, l, pl.ds(0, 1), :]
            for k in range(1, TAPS):
                acc = acc + gs[c, pl.ds(PAD - half + k, rows), :] * ptaps[c, l, pl.ds(k, 1), :]
            cv[c, pl.ds(0, rows), :] = acc + pbias[c, pl.ds(l, 1), :]
            return carry

        lax.fori_loop(0, NC, one, 0)
        parts = [cv[c, pl.ds(0, rows), :] for c in range(NC)]
        mean = jnp.sum(sum(parts[1:], parts[0]), axis=-1, keepdims=True) / C
        cent = [p - mean for p in parts]
        sq = [p * p for p in cent]
        inv = lax.rsqrt(jnp.sum(sum(sq[1:], sq[0]), axis=-1, keepdims=True) / C + epsilon)
        for c in range(NC):
            y = cent[c] * inv * plng[c, pl.ds(l, 1), :] + plns[c, pl.ds(l, 1), :]
            act[pl.ds(0, rows), pl.ds(c * 128, 128)] = (y * jax.nn.sigmoid(y)).astype(jnp.bfloat16)

    def project(l, n, a, base, rows):
        w = jnp.concatenate([wo[l, t, n].reshape(F, 128) for t in range(NC)], axis=1)
        y = lax.dot_general(a, w, (((1,), (1,)), ((), ())), preferred_element_type=jnp.float32)
        s = xs[pl.ds(base, rows), feat(n)].astype(jnp.float32)
        return (s + y).astype(jnp.bfloat16)

    def out_part(l):
        rows, base = L + 2 * E - 2 * PAD * (l + 1), PAD * (l + 1)
        a = act[pl.ds(0, rows), :]
        for n in range(D // F):
            xs[pl.ds(base, rows), pl.ds(n * F, F)] = project(l, n, a, base, rows)

    tick(0)
    land(tap_copies)
    send(tap_crossings)
    tick(1)
    tick(2)
    own_gain.wait()

    @pl.when(sp > 0)
    def _():
        to_after.wait_recv()

    @pl.when(sp < SP - 1)
    def _():
        to_before.wait_recv()

    for l in range(LAYERS):
        last = l == LAYERS - 1
        if last:
            for k in range(2):
                advance(k, 2 * LAYERS)
        for k in range(2):
            complete(k, l)
        gated_part(l)
        if l == 0:
            land(small_copies)
            land(tap_crossings)

            @pl.when(sp > 0)
            def _():
                to_before.wait_send()

            @pl.when(sp < SP - 1)
            def _():
                to_after.wait_send()

        if last:
            advance(2, 2 * LAYERS)
        else:
            tick(2 * l + 3)
        conv_part(l)
        complete(2, l)
        if not last:
            out_part(l)
            if 2 * l + 4 < 2 * LAYERS:
                tick(2 * l + 4)

    l = LAYERS - 1
    a = act[pl.ds(0, L), :]
    sends = []
    for d in (2, 1, 3, 0):
        n = lax.rem(tp + d, TP)
        y = project(l, n, a, E, L)
        if d == 0:
            out[pl.ds(tp, 1)] = y.reshape(1, L, F)
        else:
            fin[d] = y
            c = remote(fin.at[d], out.at[tp], osend.at[d], orecv.at[d], (sp, n))
            c.start()
            sends.append(c)
    for c in started:
        c.wait_send()
    for c in sends:
        c.wait()


def stacked(tokens, norm_gain, val_weight, gate_weight, conv_taps, conv_bias, ln_gain, ln_shift, out_weight):
    TP = lax.axis_size("tp")
    seqs, L, F = tokens.shape
    D = F * TP
    layers, K, width = val_weight.shape
    C = width * TP
    TAPS = conv_taps.shape[1]
    PAD = -(-(TAPS // 2) // 16) * 16
    E = PAD * layers
    rows = L + 2 * E
    bf16, f32 = jnp.bfloat16, jnp.float32
    dma = pltpu.SemaphoreType.DMA
    weight = pltpu.VMEM((layers, TP, N, N, 2, K, width), bf16)
    small = pltpu.VMEM((TP,) + conv_bias.shape, f32)
    return pl.pallas_call(
        partial(stack_kernel, (layers, L, D, C, F, K, TAPS, PAD, E)),
        out_shape=jax.ShapeDtypeStruct(tokens.shape, tokens.dtype),
        in_specs=[pl.BlockSpec(memory_space=pl.ANY)] * 9,
        out_specs=pl.BlockSpec(memory_space=pltpu.VMEM),
        scratch_shapes=[
            pltpu.VMEM((rows, D), bf16),
            weight, weight, weight,
            pltpu.VMEM(tokens.shape, bf16),
            pltpu.VMEM(norm_gain.shape, f32),
            pltpu.VMEM((TP,) + conv_taps.shape, f32),
            small, small, small,
            pltpu.VMEM(out_weight.shape, bf16),
            pltpu.VMEM((C // 128, rows, 128), f32),
            pltpu.VMEM((C // 128, rows, 128), f32),
            pltpu.VMEM((rows, C), bf16),
            pltpu.VMEM((TP, L, F), bf16),
            dma((10,)),
            dma((TP,)), dma((TP,)),
            dma((2,)), dma((2,)),
            dma((4, TP)), dma((4, TP)),
            dma((TP,)), dma((TP,)),
            dma((3, 2, 3)), dma((3, 2, 3)),
            dma((3, layers, 3)), dma((3, layers, 3)),
            dma((3, 2 * layers, 2)), dma((3, 2 * layers, 2)),
            dma((3, 2 * layers, 2)), dma((3, 2 * layers, 2)),
            dma((3, 2 * layers, 4)), dma((3, 2 * layers, 4)),
            dma((TP,)), dma((TP,)),
        ],
        compiler_params=pltpu.CompilerParams(
            collective_id=0, has_side_effects=True, vmem_limit_bytes=56 * 1024 * 1024
        ),
        name="stack",
    )(tokens, norm_gain, val_weight, gate_weight, conv_taps, conv_bias, ln_gain, ln_shift, out_weight)


def solution(mesh):
    placed = (
        P(None, "sp", "tp"),
        P(),
        P(None, "sp", "tp"),
        P(None, "sp", "tp"),
        P(None, None, "tp"),
        P(None, "tp"),
        P(None, "tp"),
        P(None, "tp"),
        P(None, "tp", "sp"),
    )
    return jax.shard_map(
        stacked, mesh=mesh, in_specs=placed, out_specs=P(None, "sp", "tp"), check_vma=False
    )
```

time: 453 us -> 65 us (0.14)
  blocking collectives: 390 us -> 0 us
  Pallas kernels: 0 us -> 61 us
  waiting for transfers between devices: 19.4 us -> 0 us
  between operations: 13.5 us -> 0.01 us
  starting transfers between devices: 11.4 us -> 0 us
  other arithmetic: 8.33 us -> 0 us
  matrix products: 7 us -> 0 us
    all_gather x16 -> x0, blocking collectives: 354 us -> none  [the longest x8 190 us: over_all(): lax.all_gather(a, axis, axis=dim, tiled=True)]
    pallas_call x0 -> x1, Pallas kernels: none -> 61 us  [stacked(): pl.pallas_call(partial(stack_kernel, (layers, L, D, C, F, K, TAPS, PAD, E...]
    psum x4 -> x0, blocking collectives: 36.1 us -> none  [shards(): lax.psum((jnp.sum(convolved, axis=-1), jnp.sum(convolved * convolved, axi...]
    reduce_scatter x4 -> x0, waiting for transfers between devices: 19.3 us -> none  [shards(): lax.psum_scatter(partial_terms.reshape(num_seqs, local_len, full_width).a...]
    ppermute x8 -> x0, starting transfers between devices: 11.3 us -> none  [the longest x4 6.13 us: with_halo(): before = lax.ppermute(last, axis, up)]
    dot_general x12 -> x0, matrix products: 7 us -> none  [the longest x4 4.66 us: project_rows(): return jnp.dot(left_rows, shard_piece, preferred_element_type=jnp.float32)]
    convert_element_type x12 -> x0, other arithmetic: 5.28 us -> none  [the longest x4 4.41 us: shards(): stream = (stream.astype(jnp.float32) + summed).astype(jnp.bfloat16)]
  transfers between devices with their start and end apart: 12 -> 0, of which waited for: 1 -> 0; matrix products, arithmetic and copies ran while one was open for 0% -> 0% of each run, Pallas kernels for 0% -> 0%
where the time goes in v1:
time: 65 us; the launch traced here: 64.8 us
  Pallas kernels  61 us (94%)
  local copies, waits for them, and re-layouts  3.81 us (6%)
    pallas_call x1, Pallas kernels, stacked(): pl.pallas_call(partial(stack_kernel, (layers, L, D, C, F, K, TAPS, PAD, E...  61 us
    unnamed x5, local copies, waits for them, and re-layouts  3.81 us

profile of v1, /device:TPU:0, one launch (start us, length us, event | category | flops | bytes accessed | tf_op | source)
XLA Modules:
  0.0 64.8 jit_solution(12224012568418446254)
XLA Ops:
  0.0 0.0 copy-start
  0.0 1.5 %copy.10.taps_h = f32[4,31,128]{2,1,0:T(8,128)} copy(f32[4,31,128]{2,0,1:T(4,128)} %param.13) | data formatting | bytes 126976 | tf_op args[4]
  1.5 0.0 copy-done
  1.5 0.8 %copy.11.outw_h = bf16[4,128,32]{2,1,0:T(8,128)(2,1)} copy(bf16[4,128,32]{1,2,0:T(8,128)(2,1)S(1)} %copy-done) | data formatting | bytes 65536 | tf_op args[8]
  2.2 61.0 %stack.1 = bf16[4,64,256]{2,1,0:T(8,128)(2,1)} custom-call(bf16[4,64,256]{2,1,0:T(8,128)(2,1)} %tok_h.1, f32[4,1024]{1,0:T(4,128)} %gain_h.1, bf16[4,32,128]{2,1,0:T(8,128)(2,1)} %val_h.1, bf16[4,32,128]{2,1,0:T(8,128)(2,1)} %gate_h.1, f32[4,31,128]{2,1,0:T(8,128)} %copy.10.taps_h, f32[4,128]{1,0:T(4,128)} %bias_h.1, f32[4,128]{1,0:T(4,128)} %lng_h.1, ...), custom_call_target="tpu_custom_call" | custom-call | tf_op jit(solution)/shard_map/stack/pallas_call | solution.py:373
  63.2 1.6 %copy.13 = bf16[4,64,256]{2,1,0:T(8,128)(2,1)} copy(bf16[4,64,256]{2,1,0:T(8,128)(2,1)} %stack.1) | data formatting | bytes 262144
Async XLA Ops:
  0.0 1.5 %copy-start = (bf16[4,128,32]{1,2,0:T(8,128)(2,1)S(1)}, bf16[4,128,32]{1,2,0:T(8,128)(2,1)}, u32[]{:S(2)}) copy-start(bf16[4,128,32]{1,2,0:T(8,128)(2,1)} %param.17) | copy-start | bytes 98308

commit v2 on v1

v2 whole, which is shorter than its diff:
```python
from functools import partial

import jax
import jax.numpy as jnp
from jax import lax
from jax.experimental import pallas as pl
from jax.experimental.pallas import tpu as pltpu
from jax.sharding import PartitionSpec as P

MESH = pl.DeviceIdType.MESH
epsilon = 1e-06

N = 4
ORDERS = (("x", "y", "z"), ("y", "z", "x"), ("z", "x", "y"))
ALL = slice(None)


def stack_kernel(
    dims, tok_h, gain_h, val_h, gate_h, taps_h, bias_h, lng_h, lns_h, outw_h, out,
    xs, wv, wg, wo, tokb, gain, ptaps, psmall, gs, cv, act, fin,
    loc, tsend, trecv, hsend, hrecv, psend, precv, wsend, ar, br, rr, cr, fr, sr, osem,
):
    LAYERS, L, D, C, F, K, TAPS, PAD, E = dims
    SP, TP = lax.axis_size("sp"), lax.axis_size("tp")
    sp, tp = lax.axis_index("sp"), lax.axis_index("tp")
    half = TAPS // 2
    me = {"x": tp, "y": lax.rem(sp // 2, N), "z": sp // (2 * N)}
    core = lax.rem(sp, 2)
    W = (wv, wg, wo)

    def device(at, c=None):
        return (at["z"] * (2 * N) + at["y"] * 2 + (core if c is None else c), at["x"])

    def along(dim, d):
        return lax.rem(me[dim] + d + N, N)

    def neighbour(dim, d):
        return device({**me, dim: along(dim, d)})

    sibling = device(me, 1 - core)
    before = (lax.rem(sp + SP - 1, SP), tp)
    after = (lax.rem(sp + 1, SP), tp)

    def remote(src, dst, ss_, rs_, to):
        return pltpu.make_async_remote_copy(
            src_ref=src, dst_ref=dst, send_sem=ss_, recv_sem=rs_,
            device_id=to, device_id_type=MESH,
        )

    def block(k, l, at, rows=ALL):
        return W[k].at[l, at["x"], at["z"], at["y"], core, rows, :]

    started = []

    def go(c):
        c.start()
        started.append(c)
        return c

    def load(src, dst, i):
        c = pltpu.make_async_copy(src, dst, loc.at[i])
        c.start()
        return c

    every = pl.ds(0, LAYERS)
    own_out = load(outw_h, block(2, every, me), 0)
    own_val = load(val_h, block(0, every, me), 1)
    own_gate = load(gate_h, block(1, every, me), 2)
    own_tok = load(tok_h, tokb, 3)

    def feat(t):
        return pl.ds(pl.multiple_of(t * F, F), F)

    own_x = load(tok_h.at[tp], xs.at[pl.ds(E, L), feat(tp)], 4)
    small_src = (bias_h, lng_h, lns_h)
    pbias, plng, plns = small_dst = [psmall.at[i] for i in range(3)]
    own_small = [load(taps_h, ptaps.at[tp, pl.ds(0, TAPS)], 5)]
    own_small += [load(s, d.at[tp], 6 + i) for i, (s, d) in enumerate(zip(small_src, small_dst))]
    own_gain = load(gain_h, gain, 9)

    barrier = pltpu.get_barrier_semaphore()
    peers = [neighbour(dim, d) for dim in "xyz" for d in (1, 2, 3)] + [before, after, sibling]
    for p in peers:
        pl.semaphore_signal(barrier, inc=1, device_id=p, device_id_type=MESH)

    with jax.named_scope("own"):
        own_out.wait()
        own_val.wait()
        own_gate.wait()
        own_tok.wait()
    with jax.named_scope("barrier"):
        pl.semaphore_wait(barrier, len(peers))

    FIRST, SECOND, RELAY, THIRD, FOURTH, ACROSS = range(6)

    def copies_of(k, kind, rs_, moves):
        return [remote(ref, ref, wsend.at[k, kind], rs_, to) for ref, to in moves]

    def wait_blocks(k, sem, *counts):
        ref = W[k].at[tuple(pl.ds(0, n) for n in counts)]
        pltpu.make_async_copy(ref, ref, sem).wait()

    def first(k, g):
        ref = block(k, 0 if g == 0 else pl.ds(1, LAYERS - 1), me)
        return copies_of(
            k, FIRST, ar.at[k, g], [(ref, neighbour(ORDERS[k][0], d)) for d in (1, -1, 2)]
        )

    def land_first(k, g):
        wait_blocks(k, ar.at[k, g], 1 if g == 0 else LAYERS - 1, 1, 1, 3, 1)

    def second(k, l):
        ref = block(k, l, {**me, ORDERS[k][0]: ALL})
        jumps = (1, -1, 2) if l == 0 else (1, -1)
        return copies_of(
            k, SECOND, br.at[k, l], [(ref, neighbour(ORDERS[k][1], d)) for d in jumps]
        )

    def land_second(k, l):
        wait_blocks(k, br.at[k, l], 1, 1, 3 if l == 0 else 2, N, 1)

    def relay(k, l):
        a, b, _ = ORDERS[k]
        return copies_of(k, RELAY, rr.at[k, l], [
            (block(k, l, {**me, a: ALL, b: along(b, -d)}, halves[j]), neighbour(b, d))
            for j, d in enumerate((1, -1))
        ])

    def land_relay(k, l):
        wait_blocks(k, rr.at[k, l], 1, 1, 1, N, 1)

    def plane(k, i, d, rows=ALL):
        a, b, e = ORDERS[k]
        at = {a: ALL, b: pl.ds(2 * (i % 2), 2), e: along(e, d) if d else me[e]}
        return block(k, i // 2, at, rows)

    def third(k, i):
        return copies_of(k, THIRD, cr.at[k, i], [
            (plane(k, i, 0), neighbour(ORDERS[k][2], d)) for d in (1, -1)
        ])

    def land_third(k, i):
        wait_blocks(k, cr.at[k, i], 1, 1, 2, N, 2)

    def fourth(k, i):
        return copies_of(k, FOURTH, fr.at[k, i], [
            (plane(k, i, -d, halves[j]), neighbour(ORDERS[k][2], d)) for j, d in enumerate((1, -1))
        ])

    def land_fourth(k, i):
        wait_blocks(k, fr.at[k, i], 1, 1, 2, N, 1)

    def across(k, i, d):
        return copies_of(k, ACROSS, sr.at[k, i // 2], [(plane(k, i, d), sibling)])

    def complete(k, l):
        wait_blocks(k, sr.at[k, l], 1, 2, N, N, 2)

    halves = (pl.ds(0, K // 2), pl.ds(K // 2, K // 2))

    def send(copies):
        for c in copies:
            c.start()

    def open_chunk(k, i):
        send(third(k, i))
        send(across(k, i, 0))

    def pass_on(k, i):
        land_third(k, i)
        send(fourth(k, i))
        send(across(k, i, -1))
        send(across(k, i, 1))

    def finish_chunk(k, i):
        land_fourth(k, i)
        send(across(k, i, 2))

    def tick(i, opened=(), relayed=None):
        with jax.named_scope(f"tick{i}"):
            for k in range(3):
                if i < 2 * LAYERS:
                    pass_on(k, i)
                if relayed is not None:
                    land_relay(k, relayed)
                for j in opened:
                    open_chunk(k, j)
                if i >= 2:
                    finish_chunk(k, i - 2)

    for k in range(3):
        send(first(k, 0))
    for k in range(3):
        send(first(k, 1))

    tok_copies = [
        remote(
            tokb.at[lax.rem(tp + d, TP)], xs.at[pl.ds(E, L), feat(tp)],
            tsend.at[0], trecv.at[0], (sp, lax.rem(tp + d, TP)),
        )
        for d in range(1, TP)
    ]
    tok_all = tokb.at[pl.ds(0, TP - 1)]
    send(tok_copies)
    with jax.named_scope("first0"):
        for k in range(3):
            land_first(k, 0)
            send(second(k, 0))
    with jax.named_scope("first1"):
        for k in range(3):
            land_first(k, 1)
            send(second(k, 1))
        for l in range(2, LAYERS):
            for k in range(3):
                send(second(k, l))
    with jax.named_scope("tokens"):
        own_x.wait()
        pltpu.make_async_copy(tok_all, tok_all, trecv.at[0]).wait()
    to_before = remote(
        xs.at[pl.ds(E, L)], xs.at[pl.ds(E + L, L)], hsend.at[0], hrecv.at[0], before
    )
    to_after = remote(xs.at[pl.ds(E, L)], xs.at[pl.ds(0, L)], hsend.at[1], hrecv.at[1], after)

    @pl.when(sp > 0)
    def _():
        to_before.start()

    @pl.when(sp < SP - 1)
    def _():
        to_after.start()

    @pl.when(sp == 0)
    def _():
        xs[pl.ds(0, E), :] = jnp.zeros((E, D), xs.dtype)

    @pl.when(sp == SP - 1)
    def _():
        xs[pl.ds(E + L, E), :] = jnp.zeros((E, D), xs.dtype)

    with jax.named_scope("second0"):
        for k in range(3):
            land_second(k, 1)
            send(relay(k, 1))
            land_second(k, 0)
            open_chunk(k, 0)
            open_chunk(k, 1)
    with jax.named_scope("second2"):
        for l in range(2, LAYERS):
            for k in range(3):
                land_second(k, l)
                send(relay(k, l))

    for c in own_small:
        c.wait()

    part = pl.ds(core * (ptaps.shape[1] // 2), ptaps.shape[1] // 2)
    for k in range(TAPS, ptaps.shape[1]):
        ptaps[pl.ds(tp, 1), k] = jnp.zeros((1,) + ptaps.shape[2:], ptaps.dtype)

    others = [lax.rem(tp + d, TP) for d in range(1, TP)]
    tap_ref = ptaps.at[tp, part]
    tap_copies = [remote(tap_ref, tap_ref, psend.at[0], precv.at[0], (sp, t)) for t in others]
    small_copies = [
        remote(d.at[tp], d.at[tp], psend.at[1], precv.at[1], (sp, t))
        for d in small_dst for t in others
    ]
    tap_crossings = [
        remote(ptaps.at[t, part], ptaps.at[t, part], psend.at[2], precv.at[2], sibling)
        for t in others
    ]
    tap_all = ptaps.at[pl.ds(0, TP - 1), part]
    small_all = psmall.at[:, pl.ds(0, TP - 1)]

    def wait_for(ref, sem):
        pltpu.make_async_copy(ref, ref, sem).wait()

    send(tap_copies)
    send(small_copies)

    NC = C // 128

    def gated_part(l):
        rows, base = L + 2 * E - 2 * PAD * l, PAD * l
        x = xs[pl.ds(base, rows), :].astype(jnp.float32)
        scaled = x * lax.rsqrt(jnp.mean(x * x, axis=-1, keepdims=True) + epsilon)
        normed = (scaled * gain[pl.ds(l, 1), :]).astype(jnp.bfloat16)
        place = sp * L - E + base + lax.broadcasted_iota(jnp.int32, (rows, 128), 0)
        inside = (place >= 0) & (place < SP * L)
        for t in range(NC):
            w = jnp.concatenate([wv[l, t].reshape(D, 128), wg[l, t].reshape(D, 128)], axis=1)
            both = jnp.dot(normed, w, preferred_element_type=jnp.float32)
            v, g = both[:, :128], both[:, 128:]
            r = (v * jax.nn.sigmoid(g)).astype(jnp.bfloat16).astype(jnp.float32)
            gs[t, pl.ds(0, rows), :] = jnp.where(inside, r, 0.0)

    def conv_part(l):
        rows = L + 2 * E - 2 * PAD * (l + 1)

        def one(c, carry):
            acc = gs[c, pl.ds(PAD - half, rows), :] * ptaps[c, 0, pl.ds(l, 1), :]
            for k in range(1, TAPS):
                acc = acc + gs[c, pl.ds(PAD - half + k, rows), :] * ptaps[c, k, pl.ds(l, 1), :]
            cv[c, pl.ds(0, rows), :] = acc + pbias[c, pl.ds(l, 1), :]
            return carry

        lax.fori_loop(0, NC, one, 0)
        parts = [cv[c, pl.ds(0, rows), :] for c in range(NC)]
        mean = jnp.sum(sum(parts[1:], parts[0]), axis=-1, keepdims=True) / C
        cent = [p - mean for p in parts]
        sq = [p * p for p in cent]
        inv = lax.rsqrt(jnp.sum(sum(sq[1:], sq[0]), axis=-1, keepdims=True) / C + epsilon)
        for c in range(NC):
            y = cent[c] * inv * plng[c, pl.ds(l, 1), :] + plns[c, pl.ds(l, 1), :]
            act[pl.ds(0, rows), pl.ds(c * 128, 128)] = (y * jax.nn.sigmoid(y)).astype(jnp.bfloat16)

    def project(l, n, a, base, rows):
        w = jnp.concatenate([wo[l, t, n].reshape(F, 128) for t in range(NC)], axis=1)
        y = lax.dot_general(a, w, (((1,), (1,)), ((), ())), preferred_element_type=jnp.float32)
        s = xs[pl.ds(base, rows), feat(n)].astype(jnp.float32)
        return (s + y).astype(jnp.bfloat16)

    def out_part(l):
        rows, base = L + 2 * E - 2 * PAD * (l + 1), PAD * (l + 1)
        a = act[pl.ds(0, rows), :]
        for n in range(D // F):
            xs[pl.ds(base, rows), pl.ds(n * F, F)] = project(l, n, a, base, rows)

    tick(0, (2, 3), 1)
    wait_for(tap_all, precv.at[0])
    send(tap_crossings)
    tick(1, (4,), 2)
    tick(2, (5,))
    tick(3, (6,), 3)
    tick(4, (7,))
    own_gain.wait()

    @pl.when(sp > 0)
    def _():
        to_after.wait_recv()

    @pl.when(sp < SP - 1)
    def _():
        to_before.wait_recv()

    for l in range(LAYERS):
        last = l == LAYERS - 1
        with jax.named_scope("arrive"):
            for k in range(2):
                complete(k, l)
        with jax.named_scope("gated"):
            gated_part(l)
        if l == 0:
            wait_for(small_all, precv.at[1])
            wait_for(tap_all, precv.at[2])

            @pl.when(sp > 0)
            def _():
                to_before.wait_send()

            @pl.when(sp < SP - 1)
            def _():
                to_after.wait_send()

        if 2 * l + 5 < 2 * LAYERS + 2:
            tick(2 * l + 5)
        with jax.named_scope("conv"):
            conv_part(l)
        with jax.named_scope("arrive2"):
            complete(2, l)
        if not last:
            with jax.named_scope("project"):
                out_part(l)
            if 2 * l + 6 < 2 * LAYERS + 2:
                tick(2 * l + 6)

    l = LAYERS - 1
    a = act[pl.ds(0, L), :]
    with jax.named_scope("finish"):
        for d in (2, 1, 3, 0):
            n = lax.rem(tp + d, TP)
            y = project(l, n, a, E, L)
            if d == 0:
                out[pl.ds(tp, 1)] = y.reshape(1, L, F)
            else:
                fin[d] = y
                send([remote(fin.at[d], out.at[tp], osem.at[0], osem.at[1], (sp, n))])
    with jax.named_scope("drain"):
        for k in range(3):
            wait_blocks(k, wsend.at[k, FIRST], LAYERS, 1, 1, 3, 1)
            wait_blocks(k, wsend.at[k, SECOND], LAYERS - 1, 1, 3, N, 1)
            wait_blocks(k, wsend.at[k, RELAY], LAYERS - 1, 1, 1, N, 1)
            wait_blocks(k, wsend.at[k, THIRD], 1, N, N, N, 2)
            wait_blocks(k, wsend.at[k, FOURTH], 1, 2, N, N, 2)
            wait_blocks(k, wsend.at[k, ACROSS], 2, N, N, N, 2)
        wait_for(tok_all, tsend.at[0])
        wait_for(tap_all, psend.at[0])
        wait_for(small_all, psend.at[1])
        wait_for(tap_all, psend.at[2])
        fin_all = fin.at[pl.ds(1, TP - 1)]
        wait_for(fin_all, osem.at[0])
        wait_for(fin_all, osem.at[1])


def stacked(tokens, norm_gain, val_weight, gate_weight, conv_taps, conv_bias, ln_gain, ln_shift, out_weight):
    TP = lax.axis_size("tp")
    seqs, L, F = tokens.shape
    D = F * TP
    layers, K, width = val_weight.shape
    C = width * TP
    TAPS = conv_taps.shape[1]
    PAD = -(-(TAPS // 2) // 16) * 16
    E = PAD * layers
    rows = L + 2 * E
    bf16, f32 = jnp.bfloat16, jnp.float32
    dma = pltpu.SemaphoreType.DMA
    weight = pltpu.VMEM((layers, TP, N, N, 2, K, width), bf16)
    return pl.pallas_call(
        partial(stack_kernel, (layers, L, D, C, F, K, TAPS, PAD, E)),
        out_shape=jax.ShapeDtypeStruct(tokens.shape, tokens.dtype),
        in_specs=[pl.BlockSpec(memory_space=pl.ANY)] * 9,
        out_specs=pl.BlockSpec(memory_space=pltpu.VMEM),
        scratch_shapes=[
            pltpu.VMEM((rows, D), bf16),
            weight, weight, weight,
            pltpu.VMEM(tokens.shape, bf16),
            pltpu.VMEM(norm_gain.shape, f32),
            pltpu.VMEM((TP, 2 * ((TAPS + 1) // 2), layers, width), f32),
            pltpu.VMEM((3, TP) + conv_bias.shape, f32),
            pltpu.VMEM((C // 128, rows, 128), f32),
            pltpu.VMEM((C // 128, rows, 128), f32),
            pltpu.VMEM((rows, C), bf16),
            pltpu.VMEM((TP, L, F), bf16),
            dma((10,)),
            dma((1,)), dma((1,)),
            dma((2,)), dma((2,)),
            dma((3,)), dma((3,)),
            dma((3, 6)),
            dma((3, 2)),
            dma((3, layers)),
            dma((3, layers)),
            dma((3, 2 * layers)),
            dma((3, 2 * layers)),
            dma((3, layers)),
            dma((2,)),
        ],
        compiler_params=pltpu.CompilerParams(
            collective_id=0, has_side_effects=True, vmem_limit_bytes=56 * 1024 * 1024
        ),
        name="stack",
    )(
        tokens, norm_gain, val_weight, gate_weight, jnp.swapaxes(conv_taps, 0, 1), conv_bias,
        ln_gain, ln_shift, jnp.swapaxes(out_weight, 1, 2),
    )


def solution(mesh):
    placed = (
        P(None, "sp", "tp"),
        P(),
        P(None, "sp", "tp"),
        P(None, "sp", "tp"),
        P(None, None, "tp"),
        P(None, "tp"),
        P(None, "tp"),
        P(None, "tp"),
        P(None, "tp", "sp"),
    )
    return jax.shard_map(
        stacked, mesh=mesh, in_specs=placed, out_specs=P(None, "sp", "tp"), check_vma=False
    )
```

time: 65 us -> 48.8 us (0.75)
  Pallas kernels: 61 us -> 46.4 us
  local copies, waits for them, and re-layouts: 3.81 us -> 1.57 us
    pallas_call x1, Pallas kernels: 61 us -> 46.4 us  [stacked(): pl.pallas_call(partial(stack_kernel, (layers, L, D, C, F, K, TAPS, PAD, E...]
    unnamed x5 -> x1, local copies, waits for them, and re-layouts: 3.81 us -> 1.57 us
where the time goes in v2:
time: 48.8 us; the launch traced here: 48 us
  Pallas kernels  46.4 us (95%)
  local copies, waits for them, and re-layouts  1.57 us (3%)
    pallas_call x1, Pallas kernels, stacked(): pl.pallas_call(partial(stack_kernel, (layers, L, D, C, F, K, TAPS, PAD, E...  46.4 us
    unnamed x1, local copies, waits for them, and re-layouts  1.57 us

profile of v2, /device:TPU:0, one launch (start us, length us, event | category | flops | bytes accessed | tf_op | source)
XLA Modules:
  0.0 48.0 jit_solution(5366540972244086095)
XLA Ops:
  0.0 46.4 %stack.1 = bf16[4,64,256]{2,1,0:T(8,128)(2,1)} custom-call(bf16[4,64,256]{2,1,0:T(8,128)(2,1)} %tok_h.1, f32[4,1024]{1,0:T(4,128)} %gain_h.1, bf16[4,32,128]{2,1,0:T(8,128)(2,1)} %val_h.1, bf16[4,32,128]{2,1,0:T(8,128)(2,1)} %gate_h.1, f32[31,4,128]{2,1,0:T(4,128)} %bitcast.2, f32[4,128]{1,0:T(4,128)} %bias_h.1, f32[4,128]{1,0:T(4,128)} %lng_h.1, ...), custom_call_target="tpu_custom_call" | custom-call | tf_op jit(solution)/shard_map/stack/pallas_call | solution.py:417
  46.4 1.6 %copy.11 = bf16[4,64,256]{2,1,0:T(8,128)(2,1)} copy(bf16[4,64,256]{2,1,0:T(8,128)(2,1)} %stack.1) | data formatting | bytes 262144
